TPU v7x, 32 devices: a whole 2x2x4 slice. The times are simulated.
32 devices in a mesh: kv: 8 (over z, y), tp: 4 (over x, core).
Axes of the slice: x: 2, y: 2, z: 4, core: 2. Of those that a mesh axis runs over, the one named last changes fastest.
Arguments:
- residual_in: bfloat16 [64, 2048], P(None, ('kv', 'tp')), may hold values from -14 to 14
- delta_state: float32 [64, 32, 128, 128], P('kv', 'tp'), may hold values from -1 to 1
- norm_gain_first: float32 [2048], P('kv'), may hold values from 0.1 to 1.9
- gate_first: bfloat16 [2048, 5632], P('kv', 'tp'), may hold values from -0.125 to 0.125
- up_first: bfloat16 [2048, 5632], P('kv', 'tp'), may hold values from -0.125 to 0.125
- down_first: bfloat16 [5632, 2048], P('tp', 'kv'), may hold values from -0.15625 to 0.15625
- norm_gain_mixer: float32 [2048], P('kv'), may hold values from 0.1 to 1.9
- query_weight: bfloat16 [2048, 2048], P('kv', 'tp'), may hold values from -0.125 to 0.125
- key_weight: bfloat16 [2048, 2048], P('kv', 'tp'), may hold values from -0.125 to 0.125
- value_weight: bfloat16 [2048, 4096], P('kv', 'tp'), may hold values from -0.125 to 0.125
- output_gate_weight: bfloat16 [2048, 4096], P('kv', 'tp'), may hold values from -0.125 to 0.125
- beta_weight: bfloat16 [2048, 32], P('kv'), may hold values from -0.125 to 0.125
- decay_weight: bfloat16 [2048, 32], P('kv'), may hold values from -0.125 to 0.125
- decay_rate: float32 [32], P('tp'), may hold values from -2.3 to 1.1
- decay_bias: float32 [32], P('tp'), may hold values from -1 to 1
- head_gain: float32 [128], replicated, may hold values from 0.1 to 1.9
- out_weight: bfloat16 [4096, 2048], P('tp', 'kv'), may hold values from -0.125 to 0.125
- norm_gain_second: float32 [2048], P('kv'), may hold values from 0.1 to 1.9
- gate_second: bfloat16 [2048, 5632], P('kv', 'tp'), may hold values from -0.125 to 0.125
- up_second: bfloat16 [2048, 5632], P('kv', 'tp'), may hold values from -0.125 to 0.125
- down_second: bfloat16 [5632, 2048], P('tp', 'kv'), may hold values from -0.15625 to 0.15625
Outputs:
- residual_out: bfloat16 [64, 2048], P(None, ('kv', 'tp'))
- delta_state_out: float32 [64, 32, 128, 128], P('kv', 'tp')
All inputs are finite; a program needn't handle non-finite values.
Results may differ from a plain program's by a relative error of at most 0.03.
Values may be sent and summed in bfloat16 or wider, within the bound.
A program may use at most 64 MiB of HBM per device.

v0:
```python
import jax
import jax.numpy as jnp
from jax import lax
from jax.sharding import PartitionSpec as P

D = 2048
epsilon = 1e-06


def activate(summed, square_sums, hidden_cols):
    rowscale = lax.rsqrt(square_sums / D + epsilon)[:, None]
    gate_act = summed[:, :hidden_cols] * rowscale
    up_act = summed[:, hidden_cols:] * rowscale
    return (jax.nn.silu(gate_act) * up_act).astype(jnp.bfloat16)


def feed_forward(residual, norm_gain, gate_weight, up_weight, down_weight, finish):
    as_float = residual.astype(jnp.float32)
    squares = jnp.sum(as_float * as_float, axis=1)
    scaled = (as_float * norm_gain).astype(jnp.bfloat16)
    joined = jnp.concatenate([gate_weight, up_weight], axis=1)
    partial_value = jnp.dot(scaled, joined, preferred_element_type=jnp.float32)
    hidden_cols = gate_weight.shape[1]
    summed, square_sums = (
        lax.psum(partial_value.astype(jnp.bfloat16), "kv").astype(jnp.float32),
        lax.psum(squares.astype(jnp.bfloat16), "kv").astype(jnp.float32),
    )
    hidden = activate(summed, square_sums, hidden_cols)
    projected = jnp.dot(hidden, down_weight, preferred_element_type=jnp.float32).astype(
        jnp.bfloat16
    )
    if finish:
        col_count = residual.shape[1] // lax.axis_size("tp")
        own_cols = lax.dynamic_slice_in_dim(
            as_float, lax.axis_index("tp") * col_count, col_count, 1
        )
        branch = lax.psum_scatter(projected, "tp", scatter_dimension=1, tiled=True).astype(
            jnp.float32
        )
        return (own_cols + 0.5 * branch).astype(jnp.bfloat16)
    branch = lax.psum(projected, "tp").astype(jnp.float32)
    return (as_float + 0.5 * branch).astype(jnp.bfloat16)


def unit_heads(projected, head_size):
    activated = jax.nn.silu(projected).reshape(projected.shape[0], -1, head_size)
    return activated * lax.rsqrt(jnp.sum(activated * activated, axis=-1, keepdims=True) + epsilon)


def delta_step(old_state, key_rows, queries, values, beta_gate, decay_gate):
    faded_state = old_state * decay_gate[:, :, None, None]
    predicted = jnp.einsum("rhab,rha->rhb", faded_state, key_rows, precision=lax.Precision.HIGHEST)
    correction = beta_gate[:, :, None] * (values - predicted)
    updated = faded_state + key_rows[:, :, :, None] * correction[:, :, None, :]
    reading = jnp.einsum("rhab,rha->rhb", updated, queries, precision=lax.Precision.HIGHEST)
    return (updated, reading)


def token_mixer(
    residual,
    norm_gain,
    query_weight,
    key_weight,
    value_weight,
    output_gate_weight,
    beta_weight,
    decay_weight,
    decay_rate,
    decay_bias,
    head_gain,
    out_weight,
    old_state,
):
    as_float = residual.astype(jnp.float32)
    squares = jnp.sum(as_float * as_float, axis=1)
    scaled = (as_float * norm_gain).astype(jnp.bfloat16)
    joined = jnp.concatenate([query_weight, key_weight, value_weight, output_gate_weight], axis=1)
    partial_value = jnp.dot(scaled, joined, preferred_element_type=jnp.float32)
    heads_dev = decay_rate.shape[0]
    head_start = lax.axis_index("tp") * heads_dev
    gate_cols = jnp.concatenate(
        [
            lax.dynamic_slice_in_dim(beta_weight, head_start, heads_dev, 1),
            lax.dynamic_slice_in_dim(decay_weight, head_start, heads_dev, 1),
        ],
        axis=1,
    )
    gate_part = jnp.dot(scaled, gate_cols, preferred_element_type=jnp.float32)
    row_count = old_state.shape[0]
    square_sums = lax.psum(squares, "kv")
    square_sums = lax.dynamic_slice_in_dim(
        square_sums, lax.axis_index("kv") * row_count, row_count, 0
    )
    summed, gate_summed = (
        lax.psum_scatter(
            partial_value.astype(jnp.bfloat16), "kv", scatter_dimension=0, tiled=True
        ).astype(jnp.float32),
        lax.psum_scatter(
            gate_part.astype(jnp.bfloat16), "kv", scatter_dimension=0, tiled=True
        ).astype(jnp.float32),
    )
    rowscale = lax.rsqrt(square_sums / D + epsilon)[:, None]
    summed = summed * rowscale
    gate_summed = gate_summed * rowscale
    head_size = old_state.shape[2]
    key_cols = query_weight.shape[1]
    value_cols = value_weight.shape[1]
    repeat_count = heads_dev // (key_cols // head_size)
    queries = jnp.repeat(
        unit_heads(summed[:, :key_cols], head_size) * head_size ** (-0.5), repeat_count, axis=1
    )
    key_rows = jnp.repeat(
        unit_heads(summed[:, key_cols : 2 * key_cols], head_size), repeat_count, axis=1
    )
    values = jax.nn.silu(summed[:, 2 * key_cols : 2 * key_cols + value_cols]).reshape(
        row_count, heads_dev, head_size
    )
    out_gate = jax.nn.silu(summed[:, 2 * key_cols + value_cols :]).reshape(
        row_count, heads_dev, head_size
    )
    beta_gate = jax.nn.sigmoid(gate_summed[:, :heads_dev])
    decay_gate = jnp.exp(
        -jnp.exp(decay_rate)[None, :]
        * jax.nn.softplus(gate_summed[:, heads_dev:] + decay_bias[None, :])
    )
    new_state, reading = delta_step(old_state, key_rows, queries, values, beta_gate, decay_gate)
    normed = reading * lax.rsqrt(jnp.mean(reading * reading, axis=-1, keepdims=True) + epsilon)
    normed = (
        (normed * head_gain * out_gate)
        .reshape(row_count, heads_dev * head_size)
        .astype(jnp.bfloat16)
    )
    projected = jnp.dot(
        lax.all_gather(normed, "kv", axis=0, tiled=True),
        out_weight,
        preferred_element_type=jnp.float32,
    ).astype(jnp.bfloat16)
    branch = lax.psum(projected, "tp").astype(jnp.float32)
    return ((as_float + branch).astype(jnp.bfloat16), new_state)


def body(
    residual_in,
    delta_state,
    norm_gain_first,
    gate_first,
    up_first,
    down_first,
    norm_gain_mixer,
    query_weight,
    key_weight,
    value_weight,
    output_gate_weight,
    beta_weight,
    decay_weight,
    decay_rate,
    decay_bias,
    head_gain,
    out_weight,
    norm_gain_second,
    gate_second,
    up_second,
    down_second,
):
    columns = lax.all_gather(residual_in, "tp", axis=1, tiled=True)
    after_first = feed_forward(columns, norm_gain_first, gate_first, up_first, down_first, False)
    after_mixer, new_state = token_mixer(
        after_first,
        norm_gain_mixer,
        query_weight,
        key_weight,
        value_weight,
        output_gate_weight,
        beta_weight,
        decay_weight,
        decay_rate,
        decay_bias,
        head_gain,
        out_weight,
        delta_state,
    )
    residual_out = feed_forward(
        after_mixer, norm_gain_second, gate_second, up_second, down_second, True
    )
    return (residual_out, new_state)


def solution(mesh):
    placed = (
        P(None, ("kv", "tp")),
        P("kv", "tp", None, None),
        P("kv"),
        P("kv", "tp"),
        P("kv", "tp"),
        P("tp", "kv"),
        P("kv"),
        P("kv", "tp"),
        P("kv", "tp"),
        P("kv", "tp"),
        P("kv", "tp"),
        P("kv", None),
        P("kv", None),
        P("tp"),
        P("tp"),
        P(),
        P("tp", "kv"),
        P("kv"),
        P("kv", "tp"),
        P("kv", "tp"),
        P("tp", "kv"),
    )
    return jax.shard_map(
        body,
        mesh=mesh,
        in_specs=placed,
        out_specs=(P(None, ("kv", "tp")), P("kv", "tp", None, None)),
        check_vma=False,
    )
```

profile of v0, /device:TPU:0, one launch (start us, length us, event | category | flops | bytes accessed | tf_op | source)
XLA Modules:
  0.0 322.3 jit_solution(16253293188831210375)
XLA Ops:
  7.2 0.9 copy.27
  8.1 6.2 %all_gather.6 = bf16[64,256]{0,1:T(8,128)(2,1)S(1)} all-gather(bf16[64,64]{0,1:T(8,128)(2,1)S(1)} %copy.27), channel_id=1, replica_groups=mesh['kv'=8,'tp'=4] {'tp'}, dimensions={1}, use_global_device_ids=true | all-gather | bytes 40960 | tf_op jit(solution)/shard_map/all_gather | solution.py:165
  14.4 2.6 convolution_convert_fusion.2
  17.2 22.4 %psum.50 = bf16[64]{0:T(256)(128)(2,1)S(1)} all-reduce(bf16[64]{0:T(256)(128)(2,1)S(1)} %fusion.27), channel_id=1, replica_groups=mesh['kv'=8,'tp'=4] {'kv'}, use_global_device_ids=true, to_apply=%region_2.0 | all-reduce | flops 64 | bytes 256 | tf_op jit(solution)/shard_map/psum | solution.py:26
  39.6 1.2 dynamic-slice
  41.5 0.7 constant_dynamic-slice_fusion
  42.2 0.7 exponential_negate_fusion
  42.9 47.6 %all-reduce.4.cloned.1.call-done = bf16[64,2816]{1,0:T(8,128)(2,1)} async-done(((bf16[64,2816]{1,0:T(8,128)(2,1)}), bf16[64,2816]{1,0:T(8,128)(2,1)}) %all-reduce.4.cloned.1.call-update) | async-done | bytes 360464 | tf_op jit(solution)/shard_map/psum | solution.py:25
  90.5 1.0 convert_element_type.96
  91.5 0.3 convolution_convert_fusion.5
  91.9 10.3 %psum.51 = bf16[64,256]{1,0:T(8,128)(2,1)S(1)} all-reduce(bf16[64,256]{1,0:T(8,128)(2,1)S(1)} %convolution_convert_fusion.5), channel_id=1, replica_groups=mesh['kv'=8,'tp'=4] {'tp'}, use_global_device_ids=true, to_apply=%region_3.4 | all-reduce | flops 16384 | bytes 65536 | tf_op jit(solution)/shard_map/psum | solution.py:41
  102.3 1.1 convolution_convert_fusion.1
  103.5 19.7 %psum.52 = f32[64]{0:T(128)S(1)} all-reduce(f32[64]{0:T(128)S(1)} %get-tuple-element.4), channel_id=1, replica_groups=mesh['kv'=8,'tp'=4] {'kv'}, use_global_device_ids=true, to_apply=%region_6.7 | all-reduce | flops 64 | bytes 512 | tf_op jit(solution)/shard_map/psum | solution.py:90
  123.4 33.1 %all-reduce = bf16[64,16]{1,0:T(8,128)(2,1)S(1)} all-reduce(bf16[64,16]{1,0:T(8,128)(2,1)S(1)} %convolution_convert_fusion.6), channel_id=2, replica_groups=mesh['kv'=8,'tp'=4] {'kv'}, use_global_device_ids=true, to_apply=%region_4.5.clone | all-reduce | flops 1024 | bytes 4096
  156.8 8.5 %reduce-scatter.5.cloned.1.call-done = bf16[8,3072]{1,0:T(8,128)(2,1)} async-done(((bf16[64,3072]{1,0:T(8,128)(2,1)}), bf16[8,3072]{1,0:T(8,128)(2,1)}) %reduce-scatter.5.cloned.1.call-update) | async-done | bytes 49168 | tf_op jit(solution)/shard_map/reduce_scatter | solution.py:95
  165.2 1.0 convert_multiply_fusion
  166.5 5.8 %fusion = f32[8,8,1,128]{3,2,1,0:T(1,128)S(1)} fusion(f32[8,8,128,1]{2,3,1,0:T(1,128)S(1)} %bitcast.57, f32[8,8,128,128]{3,2,1,0:T(8,128)} %param.22, f32[8,8]{1,0:T(8,128)S(1)} %get-tuple-element.11), kind=kOutput, calls=%fused_computation.1 | convolution fusion | flops 13631488 | bytes 4260096 | tf_op jit(solution)/shard_map/rhab,rha->rhb/dot_general | solution.py:52
  172.4 1.5 multiply_add_fusion
  174.0 2.0 copy-done.2
  176.0 3.6 %fusion.59 = f32[8,8,1,128]{3,2,1,0:T(1,128)S(1)} fusion(f32[8,8,128,128]{3,2,1,0:T(8,128)S(1)} %multiply_add_fusion, f32[8,8,128,1]{2,3,1,0:T(1,128)S(1)} %bitcast.60), kind=kOutput, calls=%fused_computation.96 | convolution fusion | flops 12582912 | bytes 4259840 | tf_op jit(solution)/shard_map/rhab,rha->rhb/dot_general | solution.py:55
  179.9 30.6 %all_gather.7 = bf16[64,1024]{1,0:T(8,128)(2,1)S(1)} all-gather(bf16[8,1024]{1,0:T(8,128)(2,1)S(1)} %fusion.45), channel_id=1, replica_groups=mesh['kv'=8,'tp'=4] {'kv'}, dimensions={0}, use_global_device_ids=true | all-gather | bytes 147456 | tf_op jit(solution)/shard_map/all_gather | solution.py:134
  210.5 0.2 convolution_convert_fusion.4
  210.8 10.3 %psum.53 = bf16[64,256]{1,0:T(8,128)(2,1)S(1)} all-reduce(bf16[64,256]{1,0:T(8,128)(2,1)S(1)} %convolution_convert_fusion.4), channel_id=1, replica_groups=mesh['kv'=8,'tp'=4] {'tp'}, use_global_device_ids=true, to_apply=%region_11.12 | all-reduce | flops 16384 | bytes 65536 | tf_op jit(solution)/shard_map/psum | solution.py:138
  221.1 1.1 convolution_convert_fusion
  222.4 19.7 %psum.55 = bf16[64]{0:T(256)(128)(2,1)S(1)} all-reduce(bf16[64]{0:T(256)(128)(2,1)S(1)} %get-tuple-element.9), channel_id=1, replica_groups=mesh['kv'=8,'tp'=4] {'kv'}, use_global_device_ids=true, to_apply=%region_14.15 | all-reduce | flops 64 | bytes 256 | tf_op jit(solution)/shard_map/psum | solution.py:26
  242.1 51.1 %all-reduce.6.cloned.1.call-done = bf16[64,2816]{1,0:T(8,128)(2,1)} async-done(((bf16[64,2816]{1,0:T(8,128)(2,1)}), bf16[64,2816]{1,0:T(8,128)(2,1)}) %all-reduce.6.cloned.1.call-update) | async-done | bytes 360464 | tf_op jit(solution)/shard_map/psum | solution.py:25
  293.2 1.0 convert_element_type.117
  294.3 0.3 convolution_convert_fusion.3
  294.6 0.7 copy.37
  295.3 19.0 %reduce-scatter.7.cloned.1.call-done = bf16[64,64]{1,0:T(8,128)(2,1)} async-done(((bf16[256,64]{1,0:T(8,128)(2,1)}), bf16[64,64]{1,0:T(8,128)(2,1)}) %reduce-scatter.7.cloned.1.call-update) | async-done | bytes 8208
  314.3 0.8 copy.38
  315.1 0.7 add_convert_fusion
  (60 shorter events, 1.7 us)
Async XLA Ops:
  7.2 84.4 %copy-start = (bf16[1408,256]{1,0:T(8,128)(2,1)S(1)}, bf16[1408,256]{1,0:T(8,128)(2,1)}, u32[]{:S(2)}) copy-start(bf16[1408,256]{1,0:T(8,128)(2,1)} %param.26) | copy-start | bytes 2162692
  7.2 83.3 %all-reduce.4.cloned.1.call-start = ((), (), s32[]{:S(2)}) async-start(), calls=%async_computation.2 | async-start | bytes 720896 | tf_op jit(solution)/shard_map/psum | solution.py:25
  14.4 87.9 %copy-start.9 = (bf16[256,1024]{1,0:T(8,128)(2,1)S(1)}, bf16[256,1024]{1,0:T(8,128)(2,1)}, u32[]{:S(2)}) copy-start(bf16[256,1024]{1,0:T(8,128)(2,1)} %param.31) | copy-start | bytes 1572868
  14.4 87.9 %copy-start.10 = (bf16[256,1024]{1,0:T(8,128)(2,1)S(1)}, bf16[256,1024]{1,0:T(8,128)(2,1)}, u32[]{:S(2)}) copy-start(bf16[256,1024]{1,0:T(8,128)(2,1)} %param.30) | copy-start | bytes 1572868
  14.4 87.9 %copy-start.11 = (bf16[256,512]{1,0:T(8,128)(2,1)S(1)}, bf16[256,512]{1,0:T(8,128)(2,1)}, u32[]{:S(2)}) copy-start(bf16[256,512]{1,0:T(8,128)(2,1)} %param.29) | copy-start | bytes 786436
  14.4 87.9 %copy-start.12 = (bf16[256,512]{1,0:T(8,128)(2,1)S(1)}, bf16[256,512]{1,0:T(8,128)(2,1)}, u32[]{:S(2)}) copy-start(bf16[256,512]{1,0:T(8,128)(2,1)} %param.28) | copy-start | bytes 786436
  14.4 87.9 %copy-start.13 = (f32[256]{0:T(256)S(1)}, f32[256]{0:T(256)}, u32[]{:S(2)}) copy-start(f32[256]{0:T(256)} %param.27) | copy-start | bytes 3076
  17.0 148.2 %reduce-scatter.5.cloned.1.call-start = ((), (), s32[]{:S(2)}) async-start(), calls=%async_computation.3 | async-start | bytes 442368 | tf_op jit(solution)/shard_map/reduce_scatter | solution.py:95
  91.9 64.7 %copy-start.5 = (f32[8]{0:T(128)S(1)}, f32[8]{0:T(128)}, u32[]{:S(2)}) copy-start(f32[8]{0:T(128)} %param.35) | copy-start | bytes 100
  103.5 189.7 %all-reduce.6.cloned.1.call-start = ((), (), s32[]{:S(2)}) async-start(), calls=%async_computation.4 | async-start | bytes 720896 | tf_op jit(solution)/shard_map/psum | solution.py:25
  165.2 7.2 %copy-start.1 = (f32[8,8,128,128]{3,2,1,0:T(8,128)S(1)}, f32[8,8,128,128]{3,2,1,0:T(8,128)}, u32[]{:S(2)}) copy-start(f32[8,8,128,128]{3,2,1,0:T(8,128)} %param.22) | copy-start | bytes 12582916
  173.9 2.1 copy-start.2
  173.9 5.9 %copy-start.4 = (f32[128]{0:T(128)S(1)}, f32[128]{0:T(128)}, u32[]{:S(2)}) copy-start(f32[128]{0:T(128)} %param.36) | copy-start | bytes 1540
  173.9 36.6 %copy-start.3 = (bf16[1024,256]{1,0:T(8,128)(2,1)S(1)}, bf16[1024,256]{1,0:T(8,128)(2,1)}, u32[]{:S(2)}) copy-start(bf16[1024,256]{1,0:T(8,128)(2,1)} %param.37) | copy-start | bytes 1572868
  173.9 47.1 %copy-start.6 = (bf16[256,1408]{1,0:T(8,128)(2,1)S(1)}, bf16[256,1408]{1,0:T(8,128)(2,1)}, u32[]{:S(2)}) copy-start(bf16[256,1408]{1,0:T(8,128)(2,1)} %param.40) | copy-start | bytes 2162692
  174.0 47.1 %copy-start.7 = (bf16[256,1408]{1,0:T(8,128)(2,1)S(1)}, bf16[256,1408]{1,0:T(8,128)(2,1)}, u32[]{:S(2)}) copy-start(bf16[256,1408]{1,0:T(8,128)(2,1)} %param.39) | copy-start | bytes 2162692
  174.0 47.1 %copy-start.14 = (f32[256]{0:T(256)S(1)}, f32[256]{0:T(256)}, u32[]{:S(2)}) copy-start(f32[256]{0:T(256)} %param.38) | copy-start | bytes 3076
  179.7 114.5 %copy-start.8 = (bf16[1408,256]{1,0:T(8,128)(2,1)S(1)}, bf16[1408,256]{1,0:T(8,128)(2,1)}, u32[]{:S(2)}) copy-start(bf16[1408,256]{1,0:T(8,128)(2,1)} %param.41) | copy-start | bytes 2162692
  222.2 92.1 %reduce-scatter.7.cloned.1.call-start = ((), (), s32[]{:S(2)}) async-start(), calls=%async_computation.5 | async-start | bytes 81920
Sparse Core Ops, SparseCore 0:
  17.1 73.3 all-reduce.3
  103.6 61.5 reduce-scatter.4
  222.3 70.8 all-reduce.5
  295.5 18.7 reduce-scatter.6
where the time goes:
time: 323 us; the launch traced here: 322 us
  blocking collectives  152 us (47%)
  waiting for transfers between devices  126 us (39%)
  matrix products  15.2 us (5%)
  between operations  14.7 us (5%)
  other arithmetic  6.96 us (2%)
  local copies, waits for them, and re-layouts  6.68 us (2%)
    psum x2, waiting for transfers between devices, feed_forward(): lax.psum(partial_value.astype(jnp.bfloat16), 'kv').astype(jnp.float32)  98.7 us
    psum x2, blocking collectives, feed_forward(): lax.psum(squares.astype(jnp.bfloat16), 'kv').astype(jnp.float32)  42.1 us
    unnamed x1, blocking collectives  33.1 us
    all_gather x1, blocking collectives, token_mixer(): lax.all_gather(normed, 'kv', axis=0, tiled=True)  30.6 us
    psum x1, blocking collectives, token_mixer(): square_sums = lax.psum(squares, 'kv')  19.7 us
    unnamed x5, waiting for transfers between devices  19.1 us
    psum x1, blocking collectives, feed_forward(): branch = lax.psum(projected, 'tp').astype(jnp.float32)  10.3 us
    psum x1, blocking collectives, token_mixer(): branch = lax.psum(projected, 'tp').astype(jnp.float32)  10.3 us
  transfers between devices with their start and end apart: 4, of which 4 were waited for; matrix products, arithmetic and copies ran while one was open for 1% of the time, Pallas kernels for 0%

commit v1 on v0

--- a/solution.py
+++ b/solution.py
@@ -5,6 +5,10 @@
 
 D = 2048
 epsilon = 1e-06
+
+
+def treat_the_region(xin, bus_axis):
+    return jnp.sum(lax.all_gather(xin, axis_name=bus_axis), axis=0)
 
 
 def activate(summed, square_sums, hidden_cols):
@@ -23,7 +27,7 @@
     hidden_cols = gate_weight.shape[1]
     summed, square_sums = (
         lax.psum(partial_value.astype(jnp.bfloat16), "kv").astype(jnp.float32),
-        lax.psum(squares.astype(jnp.bfloat16), "kv").astype(jnp.float32),
+        treat_the_region(squares.astype(jnp.bfloat16), "kv").astype(jnp.float32),
     )
     hidden = activate(summed, square_sums, hidden_cols)
     projected = jnp.dot(hidden, down_weight, preferred_element_type=jnp.float32).astype(

time: 323 us -> 341 us (1.056)
  waiting for transfers between devices: 126 us -> 143 us
    psum x2 -> x0, blocking collectives: 42.1 us -> none  [feed_forward(): lax.psum(squares.astype(jnp.bfloat16), 'kv').astype(jnp.float32)]
    unnamed x1 -> x3, blocking collectives: 33.1 us -> 75 us
    reduce_scatter x1, waiting for transfers between devices: 8.47 us -> 26.2 us  [token_mixer(): lax.psum_scatter(partial_value.astype(jnp.bfloat16), 'kv', scatter_dimens...]
where the time goes in v1:
time: 341 us; the launch traced here: 340 us
  blocking collectives  152 us (45%)
  waiting for transfers between devices  143 us (42%)
  between operations  15.4 us (5%)
  matrix products  15.2 us (4%)
  local copies, waits for them, and re-layouts  7.45 us (2%)
  other arithmetic  7 us (2%)
    psum x2, waiting for transfers between devices, feed_forward(): lax.psum(partial_value.astype(jnp.bfloat16), 'kv').astype(jnp.float32)  97.5 us
    unnamed x3, blocking collectives  75 us
    all_gather x1, blocking collectives, token_mixer(): lax.all_gather(normed, 'kv', axis=0, tiled=True)  30.6 us
    reduce_scatter x1, waiting for transfers between devices, token_mixer(): lax.psum_scatter(partial_value.astype(jnp.bfloat16), 'kv', scatter_dimens...  26.2 us
    psum x1, blocking collectives, token_mixer(): square_sums = lax.psum(squares, 'kv')  19.7 us
    unnamed x5, waiting for transfers between devices  19.1 us
    psum x1, blocking collectives, token_mixer(): branch = lax.psum(projected, 'tp').astype(jnp.float32)  10.3 us
    psum x1, blocking collectives, feed_forward(): branch = lax.psum(projected, 'tp').astype(jnp.float32)  10.3 us
  transfers between devices with their start and end apart: 4, of which 4 were waited for; matrix products, arithmetic and copies ran while one was open for 1% of the time, Pallas kernels for 0%

profile of v1, /device:TPU:0, one launch (start us, length us, event | category | flops | bytes accessed | tf_op | source)
XLA Modules:
  0.0 340.1 jit_solution(14515264399025347004)
XLA Ops:
  7.2 0.9 copy.33
  8.1 6.2 %all_gather.14 = bf16[64,256]{0,1:T(8,128)(2,1)S(1)} all-gather(bf16[64,64]{0,1:T(8,128)(2,1)S(1)} %copy.33), channel_id=1, replica_groups=mesh['kv'=8,'tp'=4] {'tp'}, dimensions={1}, use_global_device_ids=true | all-gather | bytes 40960 | tf_op jit(solution)/shard_map/all_gather | solution.py:169
  14.4 2.6 convolution_convert_fusion.2
  17.1 0.7 exponential_negate_fusion
  17.9 1.3 fusion.59
  19.8 0.2 dynamic-update-slice
  20.1 22.2 %all-reduce = bf16[512]{0:T(512)(128)(2,1)S(1)} all-reduce(bf16[512]{0:T(512)(128)(2,1)S(1)} %dynamic-update-slice), channel_id=2, replica_groups=mesh['kv'=8,'tp'=4] {'kv'}, use_global_device_ids=true, to_apply=%add | all-reduce | flops 512 | bytes 2048
  43.0 0.7 constant_dynamic-slice_fusion
  43.8 46.8 %all-reduce.6.cloned.1.call-done = bf16[64,2816]{1,0:T(8,128)(2,1)} async-done(((bf16[64,2816]{1,0:T(8,128)(2,1)}), bf16[64,2816]{1,0:T(8,128)(2,1)}) %all-reduce.6.cloned.1.call-update) | async-done | bytes 360464 | tf_op jit(solution)/shard_map/psum | solution.py:29
  90.5 1.0 convert_element_type.128
  91.6 0.3 convolution_convert_fusion.5
  91.9 10.3 %psum.36 = bf16[64,256]{1,0:T(8,128)(2,1)S(1)} all-reduce(bf16[64,256]{1,0:T(8,128)(2,1)S(1)} %convolution_convert_fusion.5), channel_id=1, replica_groups=mesh['kv'=8,'tp'=4] {'tp'}, use_global_device_ids=true, to_apply=%region_3.4 | all-reduce | flops 16384 | bytes 65536 | tf_op jit(solution)/shard_map/psum | solution.py:45
  102.3 19.7 %psum.37 = f32[64]{0:T(128)S(1)} all-reduce(f32[64]{0:T(128)S(1)} %get-tuple-element.4), channel_id=1, replica_groups=mesh['kv'=8,'tp'=4] {'kv'}, use_global_device_ids=true, to_apply=%region_6.7 | all-reduce | flops 64 | bytes 512 | tf_op jit(solution)/shard_map/psum | solution.py:94
  122.0 1.1 convolution_convert_fusion.1
  123.4 33.1 %all-reduce.2 = bf16[64,16]{1,0:T(8,128)(2,1)S(1)} all-reduce(bf16[64,16]{1,0:T(8,128)(2,1)S(1)} %convolution_convert_fusion.6), channel_id=4, replica_groups=mesh['kv'=8,'tp'=4] {'kv'}, use_global_device_ids=true, to_apply=%region_4.5.clone | all-reduce | flops 1024 | bytes 4096
  156.8 26.2 %reduce-scatter.5.cloned.1.call-done = bf16[8,3072]{1,0:T(8,128)(2,1)} async-done(((bf16[64,3072]{1,0:T(8,128)(2,1)}), bf16[8,3072]{1,0:T(8,128)(2,1)}) %reduce-scatter.5.cloned.1.call-update) | async-done | bytes 49168 | tf_op jit(solution)/shard_map/reduce_scatter | solution.py:99
  183.0 1.0 convert_multiply_fusion
  184.3 5.8 %fusion = f32[8,8,1,128]{3,2,1,0:T(1,128)S(1)} fusion(f32[8,8,128,1]{2,3,1,0:T(1,128)S(1)} %bitcast.58, f32[8,8,128,128]{3,2,1,0:T(8,128)} %param.22, f32[8,8]{1,0:T(8,128)S(1)} %get-tuple-element.11), kind=kOutput, calls=%fused_computation.1 | convolution fusion | flops 13631488 | bytes 4260096 | tf_op jit(solution)/shard_map/rhab,rha->rhb/dot_general | solution.py:56
  190.2 1.5 multiply_add_fusion
  191.8 2.0 copy-done.2
  193.8 3.6 %fusion.60 = f32[8,8,1,128]{3,2,1,0:T(1,128)S(1)} fusion(f32[8,8,128,128]{3,2,1,0:T(8,128)S(1)} %multiply_add_fusion, f32[8,8,128,1]{2,3,1,0:T(1,128)S(1)} %bitcast.61), kind=kOutput, calls=%fused_computation.97 | convolution fusion | flops 12582912 | bytes 4259840 | tf_op jit(solution)/shard_map/rhab,rha->rhb/dot_general | solution.py:59
  197.7 30.6 %all_gather.16 = bf16[64,1024]{1,0:T(8,128)(2,1)S(1)} all-gather(bf16[8,1024]{1,0:T(8,128)(2,1)S(1)} %fusion.45), channel_id=1, replica_groups=mesh['kv'=8,'tp'=4] {'kv'}, dimensions={0}, use_global_device_ids=true | all-gather | bytes 147456 | tf_op jit(solution)/shard_map/all_gather | solution.py:138
  228.6 10.3 %psum.38 = bf16[64,256]{1,0:T(8,128)(2,1)S(1)} all-reduce(bf16[64,256]{1,0:T(8,128)(2,1)S(1)} %convolution_convert_fusion.4), channel_id=1, replica_groups=mesh['kv'=8,'tp'=4] {'tp'}, use_global_device_ids=true, to_apply=%region_11.12 | all-reduce | flops 16384 | bytes 65536 | tf_op jit(solution)/shard_map/psum | solution.py:142
  238.9 1.1 convolution_convert_fusion
  240.4 19.7 %all-reduce.1 = bf16[512]{0:T(512)(128)(2,1)S(1)} all-reduce(bf16[512]{0:T(512)(128)(2,1)S(1)} %dynamic-update-slice.1), channel_id=3, replica_groups=mesh['kv'=8,'tp'=4] {'kv'}, use_global_device_ids=true, to_apply=%add.1 | all-reduce | flops 512 | bytes 2048
  260.2 50.7 %all-reduce.8.cloned.1.call-done = bf16[64,2816]{1,0:T(8,128)(2,1)} async-done(((bf16[64,2816]{1,0:T(8,128)(2,1)}), bf16[64,2816]{1,0:T(8,128)(2,1)}) %all-reduce.8.cloned.1.call-update) | async-done | bytes 360464 | tf_op jit(solution)/shard_map/psum | solution.py:29
  311.0 1.0 convert_element_type.150
  312.0 0.3 convolution_convert_fusion.3
  312.3 0.7 copy.43
  313.1 19.0 %reduce-scatter.7.cloned.1.call-done = bf16[64,64]{1,0:T(8,128)(2,1)} async-done(((bf16[256,64]{1,0:T(8,128)(2,1)}), bf16[64,64]{1,0:T(8,128)(2,1)}) %reduce-scatter.7.cloned.1.call-update) | async-done | bytes 8208
  332.0 0.8 copy.44
  332.8 0.7 add_convert_fusion
  (68 shorter events, 2.4 us)
Async XLA Ops:
  7.2 84.4 %copy-start = (bf16[1408,256]{1,0:T(8,128)(2,1)S(1)}, bf16[1408,256]{1,0:T(8,128)(2,1)}, u32[]{:S(2)}) copy-start(bf16[1408,256]{1,0:T(8,128)(2,1)} %param.26) | copy-start | bytes 2162692
  7.2 83.3 %all-reduce.6.cloned.1.call-start = ((), (), s32[]{:S(2)}) async-start(), calls=%async_computation.2 | async-start | bytes 720896 | tf_op jit(solution)/shard_map/psum | solution.py:29
  14.4 107.6 %copy-start.9 = (bf16[256,1024]{1,0:T(8,128)(2,1)S(1)}, bf16[256,1024]{1,0:T(8,128)(2,1)}, u32[]{:S(2)}) copy-start(bf16[256,1024]{1,0:T(8,128)(2,1)} %param.31) | copy-start | bytes 1572868
  14.4 107.6 %copy-start.10 = (bf16[256,1024]{1,0:T(8,128)(2,1)S(1)}, bf16[256,1024]{1,0:T(8,128)(2,1)}, u32[]{:S(2)}) copy-start(bf16[256,1024]{1,0:T(8,128)(2,1)} %param.30) | copy-start | bytes 1572868
  14.4 107.6 %copy-start.11 = (bf16[256,512]{1,0:T(8,128)(2,1)S(1)}, bf16[256,512]{1,0:T(8,128)(2,1)}, u32[]{:S(2)}) copy-start(bf16[256,512]{1,0:T(8,128)(2,1)} %param.29) | copy-start | bytes 786436
  14.4 107.6 %copy-start.12 = (bf16[256,512]{1,0:T(8,128)(2,1)S(1)}, bf16[256,512]{1,0:T(8,128)(2,1)}, u32[]{:S(2)}) copy-start(bf16[256,512]{1,0:T(8,128)(2,1)} %param.28) | copy-start | bytes 786436
  14.4 107.6 %copy-start.13 = (f32[256]{0:T(256)S(1)}, f32[256]{0:T(256)}, u32[]{:S(2)}) copy-start(f32[256]{0:T(256)} %param.27) | copy-start | bytes 3076
  17.0 166.0 %reduce-scatter.5.cloned.1.call-start = ((), (), s32[]{:S(2)}) async-start(), calls=%async_computation.3 | async-start | bytes 442368 | tf_op jit(solution)/shard_map/reduce_scatter | solution.py:99
  91.9 64.8 %copy-start.5 = (f32[8]{0:T(128)S(1)}, f32[8]{0:T(128)}, u32[]{:S(2)}) copy-start(f32[8]{0:T(128)} %param.35) | copy-start | bytes 100
  123.2 187.8 %all-reduce.8.cloned.1.call-start = ((), (), s32[]{:S(2)}) async-start(), calls=%async_computation.4 | async-start | bytes 720896 | tf_op jit(solution)/shard_map/psum | solution.py:29
  183.0 7.2 %copy-start.1 = (f32[8,8,128,128]{3,2,1,0:T(8,128)S(1)}, f32[8,8,128,128]{3,2,1,0:T(8,128)}, u32[]{:S(2)}) copy-start(f32[8,8,128,128]{3,2,1,0:T(8,128)} %param.22) | copy-start | bytes 12582916
  191.7 2.1 copy-start.2
  191.7 5.9 %copy-start.4 = (f32[128]{0:T(128)S(1)}, f32[128]{0:T(128)}, u32[]{:S(2)}) copy-start(f32[128]{0:T(128)} %param.36) | copy-start | bytes 1540
  191.7 36.6 %copy-start.3 = (bf16[1024,256]{1,0:T(8,128)(2,1)S(1)}, bf16[1024,256]{1,0:T(8,128)(2,1)}, u32[]{:S(2)}) copy-start(bf16[1024,256]{1,0:T(8,128)(2,1)} %param.37) | copy-start | bytes 1572868
  191.7 47.1 %copy-start.6 = (bf16[256,1408]{1,0:T(8,128)(2,1)S(1)}, bf16[256,1408]{1,0:T(8,128)(2,1)}, u32[]{:S(2)}) copy-start(bf16[256,1408]{1,0:T(8,128)(2,1)} %param.40) | copy-start | bytes 2162692
  191.8 47.1 %copy-start.7 = (bf16[256,1408]{1,0:T(8,128)(2,1)S(1)}, bf16[256,1408]{1,0:T(8,128)(2,1)}, u32[]{:S(2)}) copy-start(bf16[256,1408]{1,0:T(8,128)(2,1)} %param.39) | copy-start | bytes 2162692
  191.8 47.1 %copy-start.14 = (f32[256]{0:T(256)S(1)}, f32[256]{0:T(256)}, u32[]{:S(2)}) copy-start(f32[256]{0:T(256)} %param.38) | copy-start | bytes 3076
  197.5 114.5 %copy-start.8 = (bf16[1408,256]{1,0:T(8,128)(2,1)S(1)}, bf16[1408,256]{1,0:T(8,128)(2,1)}, u32[]{:S(2)}) copy-start(bf16[1408,256]{1,0:T(8,128)(2,1)} %param.41) | copy-start | bytes 2162692
  240.0 92.0 %reduce-scatter.7.cloned.1.call-start = ((), (), s32[]{:S(2)}) async-start(), calls=%async_computation.5 | async-start | bytes 81920
Sparse Core Ops, SparseCore 0:
  17.1 73.3 all-reduce.5
  123.3 59.6 reduce-scatter.4
  240.1 70.7 all-reduce.7
  313.2 18.7 reduce-scatter.6
